TPU v7x, 32 devices: a whole 2x2x4 slice. The times are simulated.
32 devices in a mesh: sp: 8 (over z, core), tp: 4 (over y, x).
Axes of the slice: x: 2, y: 2, z: 4, core: 2. Of those that a mesh axis runs over, the one named last changes fastest.
Arguments:
- tokens: bfloat16 [2, 6144, 4096], P(None, 'sp', 'tp'), may hold values from -6 to 6
- w_key: bfloat16 [4096, 2048], P(None, 'tp'), may hold values from -0.09375 to 0.09375
- w_value: bfloat16 [4096, 2048], P(None, 'tp'), may hold values from -0.09375 to 0.09375
- w_gate: bfloat16 [4096, 4, 16], replicated, may hold values from -0.09375 to 0.09375
- forget_bias: float32 [2, 16], replicated, may hold values from 3.9 to 13, as said below
- log_shift: float32 [2, 4, 16, 6144], P(None, None, 'tp', 'sp'), may hold values from -5 to 121, as said below
- new_query: bfloat16 [2, 1024, 2048], P(None, 'sp', 'tp'), may hold values from -6 to 6
Outputs:
- cache_matrix: bfloat16 [2, 2, 16, 128, 128], P(None, None, 'tp')
- cache_norm: float32 [2, 2, 16, 128], P(None, None, 'tp')
- cache_max: float32 [2, 2, 16], P(None, None, 'tp')
- first_read: bfloat16 [2, 1024, 2048], P(None, 'sp', 'tp')
Inputs may be any that keep to these rules, and one draw needn't show every extreme that they name: `forget_bias`: added to the forget gates' pre-activations, by direction and head. `log_shift`: rows 0 and 2 are added to the input gates of the two directions; rows 1 and 3 are added to the log forget gates and are never positive.
All inputs are finite; a program needn't handle non-finite values.
Results may differ from a plain program's by a relative error of at most 0.024.
Values may be sent and summed in bfloat16 or wider, within the bound.
A program may use at most 64 MiB of HBM per device.

v0:
```python
import jax
import jax.numpy as jnp
from jax import lax
from jax.sharding import PartitionSpec as P

HEAD = 128


def combined_all(array, axis, combine):
    everything = jax.tree.map(lambda part: lax.all_gather(part, axis), array)
    leading = jax.tree.map(lambda part: part[0], everything)

    def lap(k, so_far):
        return combine(so_far, jax.tree.map(lambda part: part[k], everything))

    return lax.fori_loop(1, lax.axis_size(axis), lap, leading)


def joint_max(earlier, latter):
    memory_a, norm_a, high_a = earlier
    memory_b, norm_b, high_b = latter
    highest = jnp.maximum(high_a, high_b)
    carried = jnp.exp(high_a - highest)
    own_part = jnp.exp(high_b - highest)
    memory = memory_a * carried[..., None, None] + memory_b * own_part[..., None, None]
    norm_sum = norm_a * carried[..., None] + norm_b * own_part[..., None]
    return (memory, norm_sum, highest)


def on_device(tokens, w_key, w_value, w_gate, forget_bias, log_shift, new_query):
    seq_count, seg_len, part_width = tokens.shape
    per_head = w_key.shape[1] // HEAD
    row_count = seq_count * seg_len
    first_head = lax.axis_index("tp") * per_head
    gate_cols = lax.dynamic_slice_in_dim(w_gate, first_head, per_head, 2).reshape(
        w_gate.shape[0], 4 * per_head
    )
    bias_own = lax.dynamic_slice_in_dim(forget_bias, first_head, per_head, 1)
    piece = lax.all_gather(tokens, "tp", axis=2, tiled=True)
    piece_width = piece.shape[2]
    flat_piece = piece.reshape(row_count, piece_width)
    key_sum = jnp.dot(flat_piece, w_key, preferred_element_type=jnp.float32)
    value_sum = jnp.dot(flat_piece, w_value, preferred_element_type=jnp.float32)
    gate_sum = jnp.dot(flat_piece, gate_cols, preferred_element_type=jnp.float32)
    key_rows = key_sum.astype(jnp.bfloat16).reshape(seq_count, seg_len, per_head, HEAD)
    value_rows = value_sum.astype(jnp.bfloat16).reshape(seq_count, seg_len, per_head, HEAD)
    gates = gate_sum.reshape(seq_count, seg_len, 4, per_head).transpose(0, 2, 3, 1)
    input_fwd = gates[:, 0] + log_shift[:, 0]
    forget_fwd = jax.nn.log_sigmoid(gates[:, 1] + bias_own[0][None, :, None]) + log_shift[:, 1]
    input_bwd = gates[:, 2] + log_shift[:, 2]
    forget_bwd = jax.nn.log_sigmoid(gates[:, 3] + bias_own[1][None, :, None]) + log_shift[:, 3]
    climb_fwd = jnp.cumsum(forget_fwd, axis=-1)
    total_fwd = climb_fwd[..., -1]
    weight_fwd = total_fwd[..., None] - climb_fwd + input_fwd
    climb_bwd = jnp.cumsum(forget_bwd, axis=-1)
    total_bwd = climb_bwd[..., -1]
    weight_bwd = climb_bwd - forget_bwd + input_bwd
    weights = jnp.stack([weight_fwd, weight_bwd], axis=1)
    totals = jnp.stack([total_fwd, total_bwd], axis=1)
    local_top = jnp.max(weights, axis=-1)
    scale_now = jnp.exp(weights - local_top[..., None])
    key_f = key_rows.astype(jnp.float32).transpose(0, 2, 1, 3) * HEAD ** (-0.5)
    value_f = value_rows.astype(jnp.float32).transpose(0, 2, 1, 3)
    weighted = scale_now[..., None] * key_f[:, None]
    memory = jnp.einsum("bjhld,bhle->bjhde", weighted, value_f, precision=lax.Precision.HIGHEST)
    norm_sum = jnp.sum(weighted, axis=3)
    every_total = lax.all_gather(totals[None], "sp", axis=0, tiled=True)
    my_index = lax.axis_index("sp")
    sources = jnp.arange(every_total.shape[0])[:, None, None, None]
    direction = jnp.arange(2)[None, None, :, None]
    counted = jnp.where(direction == 0, sources > my_index, sources < my_index)
    passed = jnp.sum(jnp.where(counted, every_total, 0.0), axis=0)
    total_all = jnp.sum(every_total, axis=0)
    memory_all, norm_all, top_all = combined_all(
        (memory, norm_sum, local_top + passed), "sp", joint_max
    )
    cache_max = jnp.maximum(total_all, top_all)
    rescale = jnp.exp(top_all - cache_max)
    cache_matrix = (memory_all * rescale[..., None, None]).astype(jnp.bfloat16)
    cache_norm = norm_all * rescale[..., None]
    new_count = new_query.shape[1]
    queries = new_query.reshape(seq_count, new_count, per_head, HEAD)
    numerator = jnp.einsum(
        "bthd,bjhde->bjthe", queries, cache_matrix, preferred_element_type=jnp.float32
    )
    denominator = jnp.einsum(
        "bthd,bjhd->bjth", queries.astype(jnp.float32), cache_norm, precision=lax.Precision.HIGHEST
    )
    divisor = jnp.maximum(jnp.abs(denominator), 1.0)
    first_read = jnp.sum(numerator / divisor[..., None], axis=1)
    first_read = first_read.reshape(seq_count, new_count, per_head * HEAD).astype(jnp.bfloat16)
    return (cache_matrix, cache_norm, cache_max, first_read)


def solution(mesh):
    return jax.shard_map(
        on_device,
        mesh=mesh,
        in_specs=(
            P(None, "sp", "tp"),
            P(None, "tp"),
            P(None, "tp"),
            P(),
            P(),
            P(None, None, "tp", "sp"),
            P(None, "sp", "tp"),
        ),
        out_specs=(
            P(None, None, "tp", None, None),
            P(None, None, "tp", None),
            P(None, None, "tp"),
            P(None, "sp", "tp"),
        ),
        check_vma=False,
    )
```

profile of v0, /device:TPU:0, one launch (start us, length us, event | category | flops | bytes accessed | tf_op | source)
XLA Modules:
  0.0 296.8 jit_solution(11978005785362571793)
XLA Ops:
  7.2 0.0 copy-start
  7.2 0.0 all-gather.7.cloned.1.call-start
  7.2 0.7 all-gather.7.cloned.1.call-update
  7.9 0.0 all-gather.9.cloned.1.call-start
  8.0 0.8 fusion.34
  8.8 0.1 constant_dynamic-slice_fusion.1
  8.9 0.8 constant_dynamic-slice_fusion
  9.7 125.3 %all-gather.7.cloned.1.call-done = bf16[2,768,4096]{2,1,0:T(8,128)(2,1)} async-done(((bf16[2,768,1024]{2,1,0:T(8,128)(2,1)}), bf16[2,768,4096]{2,1,0:T(8,128)(2,1)}) %all-gather.7.cloned.1.call-update) | async-done | bytes 12582928 | tf_op jit(solution)/shard_map/all_gather | solution.py:39
  135.0 7.9 %convolution_bitcast_fusion = f32[1536,16]{0,1:T(8,128)S(1)} fusion(bf16[4096,16]{0,1:T(8,128)(2,1)S(1)} %reshape.198, bf16[1536,4096]{1,0:T(8,128)(2,1)} %bitcast.91), kind=kOutput, calls=%fused_computation.16 | convolution fusion | flops 201326592 | bytes 12812288 | tf_op jit(solution)/shard_map/dot_general | solution.py:44
  142.9 0.1 reshape.199
  143.1 0.1 fusion.22
  143.2 2.3 reduce-window.14
  145.5 0.2 slice_reduce_fusion.1
  145.7 0.4 reduce-window.15
  146.0 0.1 broadcast_add_fusion.1
  146.2 0.2 slice_reduce_fusion.3
  146.3 2.3 reduce-window.16
  148.6 0.2 slice_reduce_fusion
  148.7 0.4 reduce-window.19
  149.1 0.1 broadcast_add_fusion
  149.2 0.1 fusion.30
  149.3 0.1 fusion.25
  149.4 0.1 subtract_exponential_fusion.1
  149.6 11.9 %convolution_convert_fusion.1 = bf16[1536,512]{1,0:T(8,128)(2,1)} fusion(bf16[1536,4096]{1,0:T(8,128)(2,1)} %bitcast.92, bf16[4096,512]{1,0:T(8,128)(2,1)} %param.11), kind=kOutput, calls=%fused_computation.15 | convolution fusion | flops 6443237376 | bytes 18350080 | tf_op jit(solution)/shard_map/dot_general | solution.py:43
  161.5 10.8 %convert_multiply_fusion = f32[1536,512]{1,0:T(8,128)} fusion(bf16[1536,4096]{1,0:T(8,128)(2,1)} %bitcast.93, bf16[4096,512]{1,0:T(8,128)(2,1)S(1)} %copy-done.5), kind=kOutput, calls=%fused_computation.12 | convolution fusion | flops 6444810240 | bytes 19922944 | tf_op jit(solution)/shard_map/dot_general | solution.py:42
  172.2 4.9 %mul.152 = f32[2,768,4,128]{3,2,1,0:T(4,128)} reshape(f32[1536,512]{1,0:T(8,128)} %convert_multiply_fusion) | data formatting | bytes 6291456 | tf_op jit(solution)/shard_map/mul | solution.py:62
  177.1 3.8 %copy.65 = f32[2,4,768,128]{3,2,1,0:T(8,128)} copy(f32[2,4,768,128]{3,1,2,0:T(4,128)} %bitcast.94) | data formatting | bytes 6291456 | tf_op jit(solution)/shard_map/mul | solution.py:62
  180.9 2.4 reshape.197
  183.3 2.3 copy.59
  185.6 5.3 %fusion.8 = f32[2,2,4,128,128]{3,4,1,2,0:T(8,128)S(1)} fusion(f32[2,4,768,128]{3,2,1,0:T(8,128)} %copy.65, f32[2,2,4,768]{3,1,2,0:T(2,128)S(1)} %copy.64, bf16[2,768,4,128]{1,3,2,0:T(8,128)(2,1)} %copy.59), kind=kOutput, calls=%fused_computation.18 | convolution fusion | flops 2417491968 | bytes 5816320 | tf_op jit(solution)/shard_map/bjhld,bhle->bjhde/dot_general | solution.py:65
  190.9 1.3 copy.66
  192.2 0.0 all-gather.9.cloned.1.call-update
  192.2 0.1 reshape.202
  192.3 0.1 broadcast_select_fusion
  192.4 0.2 slice_reduce_fusion.2
  192.6 12.8 %all-gather.2 = f32[16,2,4]{2,1,0:T(2,128)S(1)} all-gather(f32[2,2,4]{2,1,0:T(2,128)S(1)} %copy.68), channel_id=4, replica_groups=mesh['sp'=8,'tp'=4] {'sp'}, dimensions={0}, use_global_device_ids=true | all-gather | bytes 576 | tf_op jit(solution)/shard_map/all_gather | solution.py:67
  205.4 0.1 fusion.32
  205.5 14.4 %all-gather.3 = f32[16,2,4]{2,1,0:T(2,128)S(1)} all-gather(f32[2,2,4]{2,1,0:T(2,128)S(1)} %copy.70), channel_id=5, replica_groups=mesh['sp'=8,'tp'=4] {'sp'}, dimensions={0}, use_global_device_ids=true | all-gather | bytes 576 | tf_op jit(solution)/shard_map/all_gather | solution.py:10
  219.9 3.8 %multiply_reduce_fusion = f32[2,2,4,128]{3,1,2,0:T(2,128)S(1)} fusion(f32[2,4,768,128]{3,2,1,0:T(8,128)} %copy.65, f32[2,2,4,768]{3,1,2,0:T(2,128)S(1)} %copy.64), kind=kLoop, calls=%fused_computation.8 | loop fusion | flops 3143680 | bytes 3203072 | tf_op jit(solution)/shard_map/reduce_sum | solution.py:66
  223.7 14.5 %all-gather.1 = f32[16,2,4,128]{3,2,1,0:T(4,128)S(1)} all-gather(f32[2,2,4,128]{3,2,1,0:T(4,128)S(1)} %copy.67), channel_id=3, replica_groups=mesh['sp'=8,'tp'=4] {'sp'}, dimensions={0}, use_global_device_ids=true | all-gather | bytes 73728 | tf_op jit(solution)/shard_map/all_gather | solution.py:10
  238.3 36.6 %all-gather.9.cloned.1.call-done = f32[16,2,4,128,128]{4,3,2,1,0:T(8,128)} async-done(((f32[2,2,4,128,128]{4,3,2,1,0:T(8,128)}), f32[16,2,4,128,128]{4,3,2,1,0:T(8,128)}) %all-gather.9.cloned.1.call-update) | async-done | bytes 8388624 | tf_op jit(solution)/shard_map/all_gather | solution.py:10
  274.9 1.3 slice.88
  276.2 11.2 %while.19 = (s32[]{:T(128)}, f32[2,2,4,128,128]{4,3,2,1,0:T(8,128)S(1)}, f32[2,2,4,128]{3,2,1,0:T(4,128)S(1)}, f32[2,2,4]{2,1,0:T(2,128)S(1)}, f32[8,2,2,4]{3,2,...) while((s32[]{:T(128)}, ...), condition=%wide.region_8.9_spmd, body=%wide.region_7.8_spmd.sunk | while | flops 792629 | bytes 3171159 | solution.py:16
  276.3 0.1 fusion.47
  276.4 1.4 fusion.46
  277.9 0.1 fusion.47
  278.0 1.4 fusion.46
  279.5 0.1 fusion.47
  279.6 1.4 fusion.46
  281.1 0.1 fusion.47
  281.2 1.4 fusion.46
  282.7 0.1 fusion.47
  282.8 1.4 fusion.46
  284.3 0.1 fusion.47
  284.4 1.4 fusion.46
  285.9 0.1 fusion.47
  286.0 1.4 fusion.46
  287.4 0.6 copy.81
  288.0 0.2 multiply_convert_fusion
  288.2 0.0 copy-start.2
  288.2 0.1 broadcast_multiply_fusion
  288.3 0.5 fusion.16
  288.8 0.4 fusion.14
  289.1 0.9 copy.82
  (49 shorter events, 0.5 us)
Async XLA Ops:
  7.2 1.6 copy-start
  7.2 127.8 %all-gather.7.cloned.1.call-start = ((), (), s32[]{:S(2)}) async-start(), calls=%async_computation | async-start | bytes 15728640 | tf_op jit(solution)/shard_map/all_gather | solution.py:39
  7.9 267.0 %all-gather.9.cloned.1.call-start = ((), (), s32[]{:S(2)}) async-start(), calls=%async_computation.1 | async-start | bytes 9437184 | tf_op jit(solution)/shard_map/all_gather | solution.py:10
  135.0 14.2 %copy-start.3 = (f32[2,4,4,768]{3,2,1,0:T(4,128)S(1)}, f32[2,4,4,768]{3,2,1,0:T(4,128)}, u32[]{:S(2)}) copy-start(f32[2,4,4,768]{3,2,1,0:T(4,128)} %param.14) | copy-start | bytes 294916
  149.6 11.9 %copy-start.5 = (bf16[4096,512]{1,0:T(8,128)(2,1)S(1)}, bf16[4096,512]{1,0:T(8,128)(2,1)}, u32[]{:S(2)}) copy-start(bf16[4096,512]{1,0:T(8,128)(2,1)} %param.10) | copy-start | bytes 12582916
  185.6 6.7 %copy-start.1 = (bf16[2,128,512]{2,1,0:T(8,128)(2,1)S(1)}, bf16[2,128,512]{2,1,0:T(8,128)(2,1)}, u32[]{:S(2)}) copy-start(bf16[2,128,512]{2,1,0:T(8,128)(2,1)} %param.15) | copy-start | bytes 786436
  288.2 1.8 copy-start.2
  288.3 1.7 copy-start.4
Sparse Core Ops, SparseCore 0:
  9.8 125.0 all-gather.6
  192.3 82.5 all-gather.8
where the time goes:
time: 298 us; the launch traced here: 297 us
  waiting for transfers between devices  163 us (55%)
  blocking collectives  41.7 us (14%)
  matrix products  36.8 us (12%)
  other arithmetic  21 us (7%)
  local copies, waits for them, and re-layouts  20 us (7%)
  between operations  14.3 us (5%)
    all_gather x1, waiting for transfers between devices, on_device(): piece = lax.all_gather(tokens, 'tp', axis=2, tiled=True)  125 us
    all_gather x1, waiting for transfers between devices, combined_all(): everything = jax.tree.map(lambda part: lax.all_gather(part, axis), array)  36.6 us
    all_gather x2, blocking collectives, combined_all(): everything = jax.tree.map(lambda part: lax.all_gather(part, axis), array)  28.9 us
    all_gather x1, blocking collectives, on_device(): every_total = lax.all_gather(totals[None], 'sp', axis=0, tiled=True)  12.8 us
    dot_general x1, matrix products, on_device(): value_sum = jnp.dot(flat_piece, w_value, preferred_element_type=jnp.float32)  11.9 us
    dot_general x1, matrix products, on_device(): key_sum = jnp.dot(flat_piece, w_key, preferred_element_type=jnp.float32)  10.8 us
    add x7, other arithmetic, joint_max(): memory_a * carried[..., None, None] + memory_b * own_part[..., None, None]  10.1 us
    mul x2, local copies, waits for them, and re-layouts, on_device(): key_f = key_rows.astype(jnp.float32).transpose(0, 2, 1, 3) * HEAD ** (-0.5)  8.72 us
  transfers between devices with their start and end apart: 2, of which 2 were waited for; matrix products, arithmetic and copies ran while one was open for 2% of the time, Pallas kernels for 0%

commit v1 on v0

v1 whole, which is shorter than its diff:
```python
import functools

import jax
import jax.numpy as jnp
from jax import lax
from jax.experimental import pallas as pl
from jax.experimental.pallas import tpu as pltpu
from jax.sharding import PartitionSpec as P

HEAD = 128
CORES = 2
BF = jnp.bfloat16
F32 = jnp.float32
MESH = pl.DeviceIdType.MESH


def kernel(
    n_sp, n_tp, per_head, pad,
    tok_in, wk_in, wv_in, shift_in, wg, bias, query,
    cm_out, norm_out, max_out, read_out,
    tok, wk, wv, pk, pv, shift, shift_in2, shift_all, acc_k, acc_v, gates, kp, vp,
    stats, stat_own, norms, norm_own, pair_in, pair_own, st, rs, final, cm,
    tok_sem, wk_sem, wv_sem, local_sem, shift_sem, stat_sem, norm_sem, pair_sem, rs_sem, cm_sem,
    send_sem,
):
    s = lax.axis_index("sp")
    t = lax.axis_index("tp")
    half = n_tp // 2
    prompt = t // half
    other = 1 - prompt
    mate = lax.rem(t + half, n_tp)
    z, core = s // CORES, lax.rem(s, CORES)
    n_z = n_sp // CORES
    seg, width = tok.shape[1], tok.shape[2]
    depth = pk.shape[1]
    cols = wk.shape[2]
    sends = []
    count = [0]

    def remote(src, dst, recv, sp_to, tp_to):
        k = count[0]
        count[0] += 1
        return pltpu.make_async_remote_copy(
            src_ref=src, dst_ref=dst, send_sem=send_sem.at[k], recv_sem=recv,
            device_id=(sp_to, tp_to), device_id_type=MESH,
        )

    def send(src, dst, recv, sp_to, tp_to):
        copy = remote(src, dst, recv, sp_to, tp_to)
        copy.start()
        sends.append((None, copy))

    def send_if(cond, src, dst, recv, sp_to, tp_to):
        copy = remote(src, dst, recv, sp_to, tp_to)

        @pl.when(cond)
        def _():
            copy.start()

        sends.append((cond, copy))

    def arrived(ref, sem):
        pltpu.make_async_copy(ref, ref, sem).wait()

    barrier = pltpu.get_barrier_semaphore()
    greeted = 0
    for d in range(1, n_tp):
        pl.semaphore_signal(barrier, inc=1, device_id=(s, lax.rem(t + d, n_tp)), device_id_type=MESH)
        greeted += 1
    for d in range(1, n_sp):
        for column in (t, mate):
            pl.semaphore_signal(
                barrier, inc=1, device_id=(lax.rem(s + d, n_sp), column), device_id_type=MESH
            )
            greeted += 1

    loads = []

    def load(src, dst):
        copy = pltpu.make_async_copy(src, dst, local_sem.at[len(loads)])
        copy.start()
        loads.append(copy)

    load(tok_in.at[prompt], tok.at[t])
    load(wk_in, wk)
    load(wv_in, wv)
    load(shift_in.at[prompt], shift)
    pl.semaphore_wait(barrier, greeted)

    rows = seg // 2
    send(wk_in.at[s], pk.at[s], wk_sem.at[s], s, mate)
    send(shift_in.at[other], shift_in2, shift_sem, s, mate)
    peers = [prompt * half + lax.rem(t + d, half) for d in range(1, half)]
    for part in range(2):
        span = pl.ds(part * rows, rows)
        send(tok_in.at[other, span], tok.at[t, span], tok_sem.at[t, part], s, mate)
        for peer in peers:
            send(tok_in.at[prompt, span], tok.at[t, span], tok_sem.at[t, part], s, peer)
        if part == 0:
            send(wv_in.at[s], pv.at[s], wv_sem.at[s], s, mate)

    def relay_tokens(part):
        span = pl.ds(part * rows, rows)
        arrived(tok.at[mate, span], tok_sem.at[mate, part])
        for peer in peers:
            send(tok.at[mate, span], tok.at[mate, span], tok_sem.at[mate, part], s, peer)

    sibling = z * CORES + 1 - core

    def own_slice(held, sem):
        arrived(held.at[s], sem.at[s])
        up, down = jnp.minimum(z + 1, n_z - 1), jnp.maximum(z - 1, 0)
        send_if(z + 1 < n_z, held.at[s], held.at[s], sem.at[s], up * CORES + core, t)
        send_if(z > 0, held.at[s], held.at[s], sem.at[s], down * CORES + core, t)
        send(held.at[s], held.at[s], sem.at[s], sibling, t)

    def chain(held, sem, k):
        up, down = jnp.minimum(z + 1, n_z - 1), jnp.maximum(z - 1, 0)
        low = z - 1 - k
        low_at = jnp.maximum(low, 0) * CORES + core
        high = z + 1 + k
        high_at = jnp.minimum(high, n_z - 1) * CORES + core

        @pl.when(low >= 0)
        def _():
            arrived(held.at[low_at], sem.at[low_at])

        send_if((low >= 0) & (z + 1 < n_z), held.at[low_at], held.at[low_at], sem.at[low_at], up * CORES + core, t)
        send_if(low >= 0, held.at[low_at], held.at[low_at], sem.at[low_at], sibling, t)

        @pl.when(high < n_z)
        def _():
            arrived(held.at[high_at], sem.at[high_at])

        send_if((high < n_z) & (z > 0), held.at[high_at], held.at[high_at], sem.at[high_at], down * CORES + core, t)
        send_if(high < n_z, held.at[high_at], held.at[high_at], sem.at[high_at], sibling, t)

    tile = 256 if seg % 256 == 0 else seg
    tiles = seg // tile
    per_slot = width // depth if width >= depth else 1

    def weight_rows(ref, q):
        if width >= depth:
            return ref[pl.ds(q * per_slot, per_slot)].reshape(width, cols)
        share = depth // width
        return ref[q // share, pl.ds(pl.multiple_of(lax.rem(q, share) * width, width), width), :]

    def project(q, first):
        @pl.loop(0, tiles)
        def _(i):
            span = pl.ds(pl.multiple_of(i * tile, tile), tile)
            x = tok[q, span, :]
            ak = jnp.dot(x, weight_rows(wk, q), preferred_element_type=F32)
            av = jnp.dot(x, weight_rows(wv, q), preferred_element_type=F32)
            if first:
                acc_k[span, :] = ak
                acc_v[span, :] = av
            else:
                acc_k[span, :] += ak
                acc_v[span, :] += av

        g = lax.dot_general(wg[q], tok[q], (((1,), (1,)), ((), ())), preferred_element_type=F32)
        gates[...] = g if first else gates[...] + g

    for copy in loads:
        copy.wait()
    project(t, True)

    def peer_tokens(q):
        for part in range(2):
            span = pl.ds(part * rows, rows)
            arrived(tok.at[q, span], tok_sem.at[q, part])
        project(q, False)

    own_slice(pk, wk_sem)
    mid = [("k", k) for k in range(n_z - 1)]
    if mid:
        chain(pk, wk_sem, mid[0][1])
    relay_tokens(0)
    for _, k in mid[1:2]:
        chain(pk, wk_sem, k)
    own_slice(pv, wv_sem)
    for _, k in mid[2:]:
        chain(pk, wk_sem, k)
    for peer in peers:
        peer_tokens(peer)
    for _, k in mid[0:1]:
        chain(pv, wv_sem, k)
    relay_tokens(1)
    project(mate, False)
    for _, k in mid[1:2]:
        chain(pv, wv_sem, k)
    for peer in peers:
        peer_tokens(lax.rem(peer + half, n_tp))

    arrived(shift_in2, shift_sem)
    shift_all[...] = jnp.zeros_like(shift_all)
    for g in range(4):
        shift_all[g, 0:per_head, :] = shift[g]
        shift_all[g, per_head : 2 * per_head, :] = shift_in2[g]

    lane = lax.broadcasted_iota(jnp.int32, (pad, seg), 1)

    def log_sigmoid(v):
        return jnp.minimum(v, 0.0) - jnp.log1p(jnp.exp(-jnp.abs(v)))

    def climb(v):
        step = 1
        while step < seg:
            v = v + jnp.where(lane >= step, pltpu.roll(v, step, 1), 0.0)
            step *= 2
        return v

    def gate(g):
        return gates[g * pad : (g + 1) * pad, :]

    in_f = gate(0) + shift_all[0]
    fo_f = log_sigmoid(gate(1) + bias[0][:, 0:1]) + shift_all[1]
    in_b = gate(2) + shift_all[2]
    fo_b = log_sigmoid(gate(3) + bias[1][:, 0:1]) + shift_all[3]
    total_f = jnp.sum(fo_f, axis=1, keepdims=True)
    total_b = jnp.sum(fo_b, axis=1, keepdims=True)
    w_f = total_f - climb(fo_f) + in_f
    w_b = climb(fo_b) - fo_b + in_b
    top_f = jnp.max(w_f, axis=1, keepdims=True)
    top_b = jnp.max(w_b, axis=1, keepdims=True)
    first_lane = lax.broadcasted_iota(jnp.int32, (pad, HEAD), 1) == 0
    stat_own[0] = jnp.where(first_lane, top_f, total_f)
    stat_own[1] = jnp.where(first_lane, top_b, total_b)
    for d in range(1, n_sp):
        to = lax.rem(s + d, n_sp)
        send(stat_own, stats.at[s], stat_sem.at[s], to, t)

    def far(held, dest):
        @pl.loop(0, tiles)
        def _(i):
            span = pl.ds(pl.multiple_of(i * tile, tile), tile)
            total = jnp.zeros((tile, cols), F32)
            for q in range(n_tp):
                total += jnp.dot(tok[q, span, :], weight_rows(held, q), preferred_element_type=F32)
            dest[span, :] = total.astype(BF)

    for k in range(n_z):
        got = k * CORES + 1 - core
        arrived(pk.at[got], wk_sem.at[got])
    far(pk, kp)
    for _, k in mid[2:]:
        chain(pv, wv_sem, k)

    stats[s] = stat_own[...]
    for d in range(1, n_sp):
        frm = lax.rem(s + d, n_sp)
        arrived(stats.at[frm], stat_sem.at[frm])

    everyone = [stats[k] for k in range(n_sp)]
    total_all = [0.0, 0.0]
    after = [None] * n_sp
    running = jnp.zeros((pad, 1), F32)
    for k in reversed(range(n_sp)):
        after[k] = running
        running = running + everyone[k][0][:, 1:2]
    total_all[0] = running
    before = [None] * n_sp
    running = jnp.zeros((pad, 1), F32)
    for k in range(n_sp):
        before[k] = running
        running = running + everyone[k][1][:, 1:2]
    total_all[1] = running
    max_f, max_b = total_all
    passed_f = jnp.zeros((pad, 1), F32)
    passed_b = jnp.zeros((pad, 1), F32)
    for k in range(n_sp):
        max_f = jnp.maximum(max_f, everyone[k][0][:, 0:1] + after[k])
        max_b = jnp.maximum(max_b, everyone[k][1][:, 0:1] + before[k])
        passed_f = jnp.where(s == k, after[k], passed_f)
        passed_b = jnp.where(s == k, before[k], passed_b)
    scale_f = jnp.exp(w_f + (passed_f - max_f)) * HEAD**-0.5
    scale_b = jnp.exp(w_b + (passed_b - max_b)) * HEAD**-0.5
    both = jnp.concatenate([scale_f, scale_b], axis=0)
    scale_hi = both.astype(BF)
    scale_lo = (both - scale_hi.astype(F32)).astype(BF)

    block = st.shape[0] // n_sp
    row_of = lax.broadcasted_iota(jnp.int32, (2 * pad, HEAD), 0)
    norm_own[...] = jnp.zeros_like(norm_own)

    def head_state(index, k_h, v_h):
        k_t = k_h.astype(F32).T
        both_t = jnp.concatenate(
            [k_t * scale_f[index : index + 1, :], k_t * scale_b[index : index + 1, :]], axis=0
        ).astype(BF)
        st[index * 2 * HEAD : (index + 1) * 2 * HEAD, :] = jnp.dot(
            both_t, v_h, preferred_element_type=F32
        ).astype(BF)
        n = jnp.dot(scale_hi, k_h, preferred_element_type=F32) + jnp.dot(
            scale_lo, k_h, preferred_element_type=F32
        )
        mine = (row_of == index) | (row_of == index + pad)
        norm_own[...] = jnp.where(mine, n, norm_own[...])

    def scatter(side):
        for k in range(n_sp // 2):
            owner = side * (n_sp // 2) + k
            send_if(
                s != owner,
                st.at[pl.ds(owner * block, block)],
                rs.at[s], rs_sem.at[s], jnp.where(s == owner, sibling, owner), t,
            )

    for h in range(per_head):
        at = slice(h * HEAD, (h + 1) * HEAD)
        head_state(h, acc_k[:, at].astype(BF), acc_v[:, at].astype(BF))
    scatter(0)

    for k in range(n_z):
        got = k * CORES + 1 - core
        arrived(pv.at[got], wv_sem.at[got])
    far(pv, vp)
    for h in range(per_head):
        at = slice(h * HEAD, (h + 1) * HEAD)
        head_state(per_head + h, kp[:, at], vp[:, at])
    scatter(1)
    for d in range(1, n_sp):
        to = lax.rem(s + d, n_sp)
        send(norm_own, norms.at[s], norm_sem.at[s], to, t)
    norms[s] = norm_own[...]

    summed = st[pl.ds(pl.multiple_of(s * block, block), block), :].astype(F32)
    for d in range(1, n_sp):
        frm = lax.rem(s + d, n_sp)
        arrived(rs.at[frm], rs_sem.at[frm])
        summed = summed + rs[frm].astype(F32)
    final[...] = summed.astype(BF)

    piece = min(block, HEAD)
    mine_side = s < n_sp // 2
    column = jnp.where(mine_side, t, mate)
    for c in range(block // piece):
        start = s * block + c * piece
        head = lax.rem(start // (2 * HEAD), per_head)
        direction = lax.rem(start // HEAD, 2)
        inner = pl.ds(pl.multiple_of(lax.rem(start, HEAD), piece), piece)
        src = final.at[pl.ds(c * piece, piece)]
        dst = cm.at[prompt, direction, head, inner]
        for d in range(1, n_sp):
            send(src, dst, cm_sem.at[prompt], lax.rem(s + d, n_sp), column)
        keep = pltpu.make_async_copy(src, dst, cm_sem.at[prompt])

        @pl.when(mine_side)
        def _():
            keep.start()

        send_if(jnp.logical_not(mine_side), src, dst, cm_sem.at[prompt], s, mate)

    total_norm = jnp.zeros((2 * pad, HEAD), F32)
    for d in range(1, n_sp):
        frm = lax.rem(s + d, n_sp)
        arrived(norms.at[frm], norm_sem.at[frm])
    for k in range(n_sp):
        total_norm = total_norm + norms[k]
    pair_own[0] = total_norm
    pair_own[1, 0:pad, :] = jnp.broadcast_to(max_f, (pad, HEAD))
    pair_own[1, pad : 2 * pad, :] = jnp.broadcast_to(max_b, (pad, HEAD))
    send(pair_own, pair_in, pair_sem, s, mate)
    for j in range(2):
        norm_out[prompt, j] = pair_own[0, j * pad : j * pad + per_head, :]
        max_out[prompt, j] = pair_own[1, j * pad : j * pad + per_head, :]
    arrived(pair_in, pair_sem)
    for j in range(2):
        lo = j * pad + per_head
        norm_out[other, j] = pair_in[0, lo : lo + per_head, :]
        max_out[other, j] = pair_in[1, lo : lo + per_head, :]

    for b in range(2):
        arrived(cm.at[b], cm_sem.at[b])
    store = pltpu.make_async_copy(cm, cm_out, local_sem.at[len(loads)])
    store.start()
    for b in range(2):
        for h in range(per_head):
            at = slice(h * HEAD, (h + 1) * HEAD)
            q = query[b, :, at]
            q_f = q.astype(F32)
            total = jnp.zeros(q_f.shape, F32)
            for j in range(2):
                num = jnp.dot(q, cm[b, j, h], preferred_element_type=F32)
                den = jnp.sum(q_f * norm_out[b, j, h : h + 1, :], axis=1, keepdims=True)
                total = total + num / jnp.maximum(jnp.abs(den), 1.0)
            read_out[b, :, at] = total.astype(BF)

    for cond, copy in sends:
        if cond is None:
            copy.wait_send()
        else:
            pl.when(cond)(copy.wait_send)
    store.wait()


def on_device(n_sp, n_tp, tokens, w_key, w_value, w_gate, forget_bias, log_shift, new_query):
    seqs, seg, width = tokens.shape
    depth_all, cols = w_key.shape
    per_head = cols // HEAD
    pad = -(-2 * per_head // 8) * 8
    t = lax.axis_index("tp")
    mate = lax.rem(t + n_tp // 2, n_tp)

    def pair(array, axis):
        parts = [
            lax.dynamic_slice_in_dim(array, k * per_head, per_head, axis) for k in (t, mate)
        ]
        widths = [(0, 0)] * array.ndim
        widths[axis] = (0, pad - 2 * per_head)
        return jnp.pad(jnp.concatenate(parts, axis=axis), widths)

    gate_cols = pair(w_gate, 2).reshape(n_tp, width, 4 * pad).transpose(0, 2, 1)
    bias = jnp.broadcast_to(pair(forget_bias, 1)[..., None], (2, pad, HEAD))
    depth = depth_all // n_sp
    slabs = (n_sp, depth, cols)
    state_rows = 2 * per_head * 2 * HEAD
    block = state_rows // n_sp
    n_z = n_sp // CORES
    half = n_tp // 2
    n_send = (
        2 + 2 * half + 1 + 2 * (half - 1) + 2 * 3 + 2 * (n_z - 1) * 4
        + 3 * (n_sp - 1) + n_sp + max(1, block // HEAD) * n_sp + 4
    )
    vmem = pltpu.VMEM
    dma = pltpu.SemaphoreType.DMA
    new = new_query.shape[1]
    any_spec = pl.BlockSpec(memory_space=pl.ANY)
    vm_spec = pl.BlockSpec(memory_space=vmem)
    cm, norm, top, read = pl.pallas_call(
        functools.partial(kernel, n_sp, n_tp, per_head, pad),
        out_shape=(
            jax.ShapeDtypeStruct((seqs, 2, per_head, HEAD, HEAD), BF),
            jax.ShapeDtypeStruct((seqs, 2, per_head, HEAD), F32),
            jax.ShapeDtypeStruct((seqs, 2, per_head, HEAD), F32),
            jax.ShapeDtypeStruct((seqs, new, cols), BF),
        ),
        in_specs=[any_spec] * 4 + [vm_spec] * 3,
        out_specs=(any_spec, vm_spec, vm_spec, vm_spec),
        scratch_shapes=[
            vmem((n_tp, seg, width), BF),
            vmem(slabs, BF), vmem(slabs, BF), vmem(slabs, BF), vmem(slabs, BF),
            vmem((4, per_head, seg), F32), vmem((4, per_head, seg), F32), vmem((4, pad, seg), F32),
            vmem((seg, cols), F32), vmem((seg, cols), F32), vmem((4 * pad, seg), F32),
            vmem((seg, cols), BF), vmem((seg, cols), BF),
            vmem((n_sp, 2, pad, HEAD), F32), vmem((2, pad, HEAD), F32),
            vmem((n_sp, 2 * pad, HEAD), F32), vmem((2 * pad, HEAD), F32),
            vmem((2, 2 * pad, HEAD), F32), vmem((2, 2 * pad, HEAD), F32),
            vmem((state_rows, HEAD), BF), vmem((n_sp, block, HEAD), BF), vmem((block, HEAD), BF),
            vmem((seqs, 2, per_head, HEAD, HEAD), BF),
            dma((n_tp, 2)), dma((n_sp,)), dma((n_sp,)), dma((6,)), dma, dma((n_sp,)), dma((n_sp,)),
            dma, dma((n_sp,)), dma((2,)), dma((n_send,)),
        ],
        compiler_params=pltpu.CompilerParams(
            collective_id=0, has_side_effects=True, vmem_limit_bytes=60 * 2**20
        ),
    )(
        tokens, w_key.reshape(slabs), w_value.reshape(slabs), log_shift, gate_cols, bias, new_query
    )
    return cm, norm, top[..., 0], read


def solution(mesh):
    return jax.shard_map(
        functools.partial(on_device, mesh.shape["sp"], mesh.shape["tp"]),
        mesh=mesh,
        in_specs=(
            P(None, "sp", "tp"),
            P(None, "tp"),
            P(None, "tp"),
            P(),
            P(),
            P(None, None, "tp", "sp"),
            P(None, "sp", "tp"),
        ),
        out_specs=(
            P(None, None, "tp", None, None),
            P(None, None, "tp", None),
            P(None, None, "tp"),
            P(None, "sp", "tp"),
        ),
        check_vma=False,
    )
```

time: 298 us -> 141 us (0.47)
  waiting for transfers between devices: 163 us -> 0 us
  Pallas kernels: 0 us -> 130 us
  blocking collectives: 41.7 us -> 0 us
  matrix products: 36.8 us -> 0 us
  other arithmetic: 21 us -> 0.21 us
  between operations: 14.3 us -> 0.67 us
  local copies, waits for them, and re-layouts: 20 us -> 9.85 us
    all_gather x2 -> x0, waiting for transfers between devices: 162 us -> none  [the longest x1 125 us: on_device(): piece = lax.all_gather(tokens, 'tp', axis=2, tiled=True)]
    pallas_call x0 -> x1, Pallas kernels: none -> 130 us  [on_device(): pl.pallas_call(functools.partial(kernel, n_sp, n_tp, per_head, pad), out_...]
    all_gather x3 -> x0, blocking collectives: 41.7 us -> none  [the longest x2 28.9 us: combined_all(): everything = jax.tree.map(lambda part: lax.all_gather(part, axis), array)]
    dot_general x6 -> x0, matrix products: 36.8 us -> none  [the longest x1 11.9 us: on_device(): value_sum = jnp.dot(flat_piece, w_value, preferred_element_type=jnp.float32)]
    add x17 -> x0, other arithmetic: 11 us -> none  [the longest x7 10.1 us: joint_max(): memory_a * carried[..., None, None] + memory_b * own_part[..., None, None]]
    mul x2 -> x0, local copies, waits for them, and re-layouts: 8.72 us -> none  [on_device(): key_f = key_rows.astype(jnp.float32).transpose(0, 2, 1, 3) * HEAD ** (-0.5)]
    another operation x7 -> x0, other arithmetic: 5.44 us -> none
    reduce_sum x2 -> x0, other arithmetic: 3.88 us -> none  [the longest x1 3.79 us: on_device(): norm_sum = jnp.sum(weighted, axis=3)]
  transfers between devices with their start and end apart: 2 -> 0, of which waited for: 2 -> 0; matrix products, arithmetic and copies ran while one was open for 2% -> 0% of each run, Pallas kernels for 0% -> 0%
where the time goes in v1:
time: 141 us; the launch traced here: 140 us
  Pallas kernels  130 us (92%)
  local copies, waits for them, and re-layouts  9.85 us (7%)
    pallas_call x1, Pallas kernels, on_device(): pl.pallas_call(functools.partial(kernel, n_sp, n_tp, per_head, pad), out_...  130 us
    unnamed x3, local copies, waits for them, and re-layouts  4.85 us

profile of v1, /device:TPU:0, one launch (start us, length us, event | category | flops | bytes accessed | tf_op | source)
XLA Modules:
  0.0 140.3 jit_solution(16596735284741091701)
XLA Ops:
  0.6 0.8 constant_dynamic-slice_fusion.1
  1.5 0.1 pad_maximum_fusion.1
  1.6 0.7 broadcast_in_dim.2.bias
  2.2 1.2 constant_dynamic-slice_fusion.3
  3.4 0.1 pad_maximum_fusion
  3.5 0.2 reshape.20
  3.7 0.8 copy.13
  4.5 129.6 %shard_map.102 = (bf16[2,2,4,128,128]{4,3,2,1,0:T(8,128)(2,1)}, f32[2,2,4,128]{3,2,1,0:T(4,128)}, f32[2,2,4,128]{3,2,1,0:T(4,128)}, bf16[2,128,512]{2,1,0:T(8,128)(2,1)}) custom-call(bf16[2,768,1024]{2,1,0:T(8,128)(2,1)} %tok_in.1, bf16[8,512,512]{2,1,0:T(8,128)(2,1)} %bitcast.7, bf16[8,512,512]{2,1,0:T(8,128)(2,1)} %bitcast.8, f32[2,4,4,768]{3,2,1,0:T(4,128)} %shift_in.1, ...), custom_call_target="tpu_custom_call" | custom-call | tf_op jit(solution)/shard_map/pallas_call | solution.py:431
  134.1 1.4 slice_reduce_fusion
  135.5 1.9 %copy.17 = bf16[2,2,4,128,128]{4,3,2,1,0:T(8,128)(2,1)} copy(bf16[2,2,4,128,128]{4,3,2,1,0:T(8,128)(2,1)} %get-tuple-element.20) | data formatting | bytes 1048576
  137.3 1.3 copy.18
  138.6 1.7 %copy.19 = bf16[2,128,512]{2,1,0:T(8,128)(2,1)} copy(bf16[2,128,512]{2,1,0:T(8,128)(2,1)} %get-tuple-element.23) | data formatting | bytes 524288

commit v2 on v1

--- a/solution.py
+++ b/solution.py
@@ -16,11 +16,11 @@
 
 def kernel(
     n_sp, n_tp, per_head, pad,
-    tok_in, wk_in, wv_in, shift_in, wg, bias, query,
-    cm_out, norm_out, max_out, read_out,
-    tok, wk, wv, pk, pv, shift, shift_in2, shift_all, acc_k, acc_v, gates, kp, vp,
+    tok_in, wk_in, wv_in, shift_in, wg, bias,
+    cm_out, norm_out, max_out,
+    tok, wk, wv, far_w, shift, shift_in2, acc_k, acc_v, gates, gate_rows, kp, vp,
     stats, stat_own, norms, norm_own, pair_in, pair_own, st, rs, final, cm,
-    tok_sem, wk_sem, wv_sem, local_sem, shift_sem, stat_sem, norm_sem, pair_sem, rs_sem, cm_sem,
+    tok_sem, far_sem, local_sem, shift_sem, stat_sem, norm_sem, pair_sem, rs_sem, cm_sem,
     send_sem,
 ):
     s = lax.axis_index("sp")
@@ -32,7 +32,6 @@
     z, core = s // CORES, lax.rem(s, CORES)
     n_z = n_sp // CORES
     seg, width = tok.shape[1], tok.shape[2]
-    depth = pk.shape[1]
     cols = wk.shape[2]
     sends = []
     count = [0]
@@ -87,17 +86,44 @@
     load(shift_in.at[prompt], shift)
     pl.semaphore_wait(barrier, greeted)
 
-    rows = seg // 2
-    send(wk_in.at[s], pk.at[s], wk_sem.at[s], s, mate)
+    uneven = n_z >= 4
+    slots = 5 if uneven else 4
+    units = 2 * n_z
+
+    def flag(cond):
+        return jnp.where(cond, 1, 0)
+
+    def share(o):
+        if not uneven:
+            return 4, 4 * o
+        extra = flag(o == 0) + flag(o == n_z - 1) - flag(o == 1) - flag(o == n_z - 2)
+        return 4 + extra, 4 * o + flag(o == 1) - flag(o == n_z - 1)
+
+    def slab_of(i):
+        i = jnp.clip(i, 0, 2 * units - 1)
+        return i // units, lax.rem(i, units) * CORES + core
+
+    sibling = z * CORES + 1 - core
+    above = jnp.minimum(z + 1, n_z - 1) * CORES + core
+    below = jnp.maximum(z - 1, 0) * CORES + core
+    own_count, own_start = share(z)
+    for j in range(slots):
+        kv, at = slab_of(own_start + j)
+        for which, source in ((0, wk_in), (1, wv_in)):
+            send_if(
+                (j < own_count) & (kv == which), source.at[at], far_w.at[which, at],
+                far_sem.at[which, at], s, mate,
+            )
+
     send(shift_in.at[other], shift_in2, shift_sem, s, mate)
+    chunks = tok_sem.shape[1]
+    rows = seg // chunks
     peers = [prompt * half + lax.rem(t + d, half) for d in range(1, half)]
-    for part in range(2):
+    for part in range(chunks):
         span = pl.ds(part * rows, rows)
         send(tok_in.at[other, span], tok.at[t, span], tok_sem.at[t, part], s, mate)
         for peer in peers:
             send(tok_in.at[prompt, span], tok.at[t, span], tok_sem.at[t, part], s, peer)
-        if part == 0:
-            send(wv_in.at[s], pv.at[s], wv_sem.at[s], s, mate)
 
     def relay_tokens(part):
         span = pl.ds(part * rows, rows)
@@ -105,45 +131,35 @@
         for peer in peers:
             send(tok.at[mate, span], tok.at[mate, span], tok_sem.at[mate, part], s, peer)
 
-    sibling = z * CORES + 1 - core
-
-    def own_slice(held, sem):
-        arrived(held.at[s], sem.at[s])
-        up, down = jnp.minimum(z + 1, n_z - 1), jnp.maximum(z - 1, 0)
-        send_if(z + 1 < n_z, held.at[s], held.at[s], sem.at[s], up * CORES + core, t)
-        send_if(z > 0, held.at[s], held.at[s], sem.at[s], down * CORES + core, t)
-        send(held.at[s], held.at[s], sem.at[s], sibling, t)
-
-    def chain(held, sem, k):
-        up, down = jnp.minimum(z + 1, n_z - 1), jnp.maximum(z - 1, 0)
-        low = z - 1 - k
-        low_at = jnp.maximum(low, 0) * CORES + core
-        high = z + 1 + k
-        high_at = jnp.minimum(high, n_z - 1) * CORES + core
-
-        @pl.when(low >= 0)
+    def pass_on(o, j, up, down):
+        number, start = share(o)
+        valid = (o >= 0) & (o < n_z) & (j < number)
+        kv, at = slab_of(start + j)
+        here, sem = far_w.at[kv, at], far_sem.at[kv, at]
+
+        @pl.when(valid)
         def _():
-            arrived(held.at[low_at], sem.at[low_at])
-
-        send_if((low >= 0) & (z + 1 < n_z), held.at[low_at], held.at[low_at], sem.at[low_at], up * CORES + core, t)
-        send_if(low >= 0, held.at[low_at], held.at[low_at], sem.at[low_at], sibling, t)
-
-        @pl.when(high < n_z)
-        def _():
-            arrived(held.at[high_at], sem.at[high_at])
-
-        send_if((high < n_z) & (z > 0), held.at[high_at], held.at[high_at], sem.at[high_at], down * CORES + core, t)
-        send_if(high < n_z, held.at[high_at], held.at[high_at], sem.at[high_at], sibling, t)
+            arrived(here, sem)
+
+        if up:
+            send_if(valid & (z + 1 < n_z), here, here, sem, above, t)
+        if down:
+            send_if(valid & (z > 0), here, here, sem, below, t)
+        send_if(valid, here, here, sem, sibling, t)
+
+    def stage(r, j):
+        if r == 0:
+            pass_on(z, j, True, True)
+        else:
+            pass_on(z - r, j, True, False)
+            pass_on(z + r, j, False, True)
 
     tile = 256 if seg % 256 == 0 else seg
     tiles = seg // tile
-    per_slot = width // depth if width >= depth else 1
+    per_slot = wk.shape[0] // n_tp
 
     def weight_rows(ref, q):
-        if width >= depth:
-            return ref[pl.ds(q * per_slot, per_slot)].reshape(width, cols)
-        share = depth // width
-        return ref[q // share, pl.ds(pl.multiple_of(lax.rem(q, share) * width, width), width), :]
+        return ref[pl.ds(q * per_slot, per_slot)].reshape(width, cols)
 
     def project(q, first):
         @pl.loop(0, tiles)
@@ -159,45 +175,63 @@
                 acc_k[span, :] += ak
                 acc_v[span, :] += av
 
-        g = lax.dot_general(wg[q], tok[q], (((1,), (1,)), ((), ())), preferred_element_type=F32)
+        g = lax.dot_general(wg[:, pl.ds(pl.multiple_of(q * width, width), width)], tok[q], (((1,), (1,)), ((), ())), preferred_element_type=F32)
         gates[...] = g if first else gates[...] + g
 
+    stage(0, 0)
     for copy in loads:
         copy.wait()
     project(t, True)
 
     def peer_tokens(q):
-        for part in range(2):
+        for part in range(chunks):
             span = pl.ds(part * rows, rows)
             arrived(tok.at[q, span], tok_sem.at[q, part])
         project(q, False)
 
-    own_slice(pk, wk_sem)
-    mid = [("k", k) for k in range(n_z - 1)]
-    if mid:
-        chain(pk, wk_sem, mid[0][1])
-    relay_tokens(0)
-    for _, k in mid[1:2]:
-        chain(pk, wk_sem, k)
-    own_slice(pv, wv_sem)
-    for _, k in mid[2:]:
-        chain(pk, wk_sem, k)
-    for peer in peers:
-        peer_tokens(peer)
-    for _, k in mid[0:1]:
-        chain(pv, wv_sem, k)
-    relay_tokens(1)
+    order = sorted(
+        ((r, j) for r in range(n_z) for j in range(slots)), key=lambda x: (x[0] + x[1], x[0])
+    )
+    place = [int(len(order) * (0.5 + 0.4 * part / chunks)) for part in range(chunks)]
+    for k, (r, j) in enumerate(order):
+        if (r, j) != (0, 0):
+            stage(r, j)
+        for part in range(chunks):
+            if place[part] == k:
+                relay_tokens(part)
+        if k == place[chunks // 2]:
+            for peer in peers:
+                peer_tokens(peer)
     project(mate, False)
-    for _, k in mid[1:2]:
-        chain(pv, wv_sem, k)
     for peer in peers:
         peer_tokens(lax.rem(peer + half, n_tp))
 
     arrived(shift_in2, shift_sem)
-    shift_all[...] = jnp.zeros_like(shift_all)
+    heads_all = n_tp * per_head
+    eye = lax.broadcasted_iota(jnp.int32, (heads_all, heads_all), 0) == lax.broadcasted_iota(
+        jnp.int32, (heads_all, heads_all), 1
+    )
+    gate_rows[...] = jnp.zeros_like(gate_rows)
     for g in range(4):
-        shift_all[g, 0:per_head, :] = shift[g]
-        shift_all[g, per_head : 2 * per_head, :] = shift_in2[g]
+        rows_g = gates[g * heads_all : (g + 1) * heads_all, :]
+        if g % 2:
+            rows_g = rows_g + jnp.sum(
+                jnp.where(eye, bias[g // 2 : g // 2 + 1, :], 0.0), axis=1, keepdims=True
+            )
+        for k in range(n_tp):
+            @pl.when(t == k)
+            def _():
+                gate_rows[g, 0:per_head, :] = rows_g[k * per_head : (k + 1) * per_head]
+
+            @pl.when(mate == k)
+            def _():
+                gate_rows[g, per_head : 2 * per_head, :] = rows_g[k * per_head : (k + 1) * per_head]
+
+    def shifts(g):
+        parts = [shift[g], shift_in2[g]]
+        if pad > 2 * per_head:
+            parts.append(jnp.zeros((pad - 2 * per_head, seg), F32))
+        return jnp.concatenate(parts, axis=0)
 
     lane = lax.broadcasted_iota(jnp.int32, (pad, seg), 1)
 
@@ -211,13 +245,10 @@
             step *= 2
         return v
 
-    def gate(g):
-        return gates[g * pad : (g + 1) * pad, :]
-
-    in_f = gate(0) + shift_all[0]
-    fo_f = log_sigmoid(gate(1) + bias[0][:, 0:1]) + shift_all[1]
-    in_b = gate(2) + shift_all[2]
-    fo_b = log_sigmoid(gate(3) + bias[1][:, 0:1]) + shift_all[3]
+    in_f = gate_rows[0] + shifts(0)
+    fo_f = log_sigmoid(gate_rows[1]) + shifts(1)
+    in_b = gate_rows[2] + shifts(2)
+    fo_b = log_sigmoid(gate_rows[3]) + shifts(3)
     total_f = jnp.sum(fo_f, axis=1, keepdims=True)
     total_b = jnp.sum(fo_b, axis=1, keepdims=True)
     w_f = total_f - climb(fo_f) + in_f
@@ -240,12 +271,13 @@
                 total += jnp.dot(tok[q, span, :], weight_rows(held, q), preferred_element_type=F32)
             dest[span, :] = total.astype(BF)
 
-    for k in range(n_z):
-        got = k * CORES + 1 - core
-        arrived(pk.at[got], wk_sem.at[got])
-    far(pk, kp)
-    for _, k in mid[2:]:
-        chain(pv, wv_sem, k)
+    def swapped(kv):
+        for k in range(units):
+            got = k * CORES + 1 - core
+            arrived(far_w.at[kv, got], far_sem.at[kv, got])
+
+    swapped(0)
+    far(far_w.at[0], kp)
 
     stats[s] = stat_own[...]
     for d in range(1, n_sp):
@@ -312,10 +344,8 @@
         head_state(h, acc_k[:, at].astype(BF), acc_v[:, at].astype(BF))
     scatter(0)
 
-    for k in range(n_z):
-        got = k * CORES + 1 - core
-        arrived(pv.at[got], wv_sem.at[got])
-    far(pv, vp)
+    swapped(1)
+    far(far_w.at[1], vp)
     for h in range(per_head):
         at = slice(h * HEAD, (h + 1) * HEAD)
         head_state(per_head + h, kp[:, at], vp[:, at])
@@ -375,7 +405,24 @@
         arrived(cm.at[b], cm_sem.at[b])
     store = pltpu.make_async_copy(cm, cm_out, local_sem.at[len(loads)])
     store.start()
-    for b in range(2):
+    for cond, copy in sends:
+        if cond is None:
+            copy.wait_send()
+        else:
+            pl.when(cond)(copy.wait_send)
+    store.wait()
+
+
+def finish(cm, norm, top, query, cm_out, norm_out, max_out, read_out):
+    seqs, _, per_head = norm.shape[:3]
+    row = lax.broadcasted_iota(jnp.int32, (per_head, HEAD), 0)
+    diagonal = row == lax.broadcasted_iota(jnp.int32, (per_head, HEAD), 1)
+    cm_out[...] = cm[...]
+    norm_out[...] = norm[...]
+    for b in range(seqs):
+        for j in range(2):
+            line = jnp.sum(jnp.where(diagonal, top[b, j], 0.0), axis=0, keepdims=True)
+            max_out[b, j : j + 1, :] = line[:, 0:per_head]
         for h in range(per_head):
             at = slice(h * HEAD, (h + 1) * HEAD)
             q = query[b, :, at]
@@ -383,16 +430,9 @@
             total = jnp.zeros(q_f.shape, F32)
             for j in range(2):
                 num = jnp.dot(q, cm[b, j, h], preferred_element_type=F32)
-                den = jnp.sum(q_f * norm_out[b, j, h : h + 1, :], axis=1, keepdims=True)
+                den = jnp.sum(q_f * norm[b, j, h : h + 1, :], axis=1, keepdims=True)
                 total = total + num / jnp.maximum(jnp.abs(den), 1.0)
             read_out[b, :, at] = total.astype(BF)
-
-    for cond, copy in sends:
-        if cond is None:
-            copy.wait_send()
-        else:
-            pl.when(cond)(copy.wait_send)
-    store.wait()
 
 
 def on_device(n_sp, n_tp, tokens, w_key, w_value, w_gate, forget_bias, log_shift, new_query):
@@ -400,27 +440,16 @@
     depth_all, cols = w_key.shape
     per_head = cols // HEAD
     pad = -(-2 * per_head // 8) * 8
-    t = lax.axis_index("tp")
-    mate = lax.rem(t + n_tp // 2, n_tp)
-
-    def pair(array, axis):
-        parts = [
-            lax.dynamic_slice_in_dim(array, k * per_head, per_head, axis) for k in (t, mate)
-        ]
-        widths = [(0, 0)] * array.ndim
-        widths[axis] = (0, pad - 2 * per_head)
-        return jnp.pad(jnp.concatenate(parts, axis=axis), widths)
-
-    gate_cols = pair(w_gate, 2).reshape(n_tp, width, 4 * pad).transpose(0, 2, 1)
-    bias = jnp.broadcast_to(pair(forget_bias, 1)[..., None], (2, pad, HEAD))
-    depth = depth_all // n_sp
-    slabs = (n_sp, depth, cols)
+    heads_all = w_gate.shape[2]
+    gate_t = w_gate.transpose(1, 2, 0).reshape(4 * heads_all, depth_all)
+    slabs = (2 * n_sp, depth_all // (2 * n_sp), cols)
     state_rows = 2 * per_head * 2 * HEAD
     block = state_rows // n_sp
     n_z = n_sp // CORES
     half = n_tp // 2
+    chunks = 4
     n_send = (
-        2 + 2 * half + 1 + 2 * (half - 1) + 2 * 3 + 2 * (n_z - 1) * 4
+        10 + 1 + chunks * (2 * half - 1) + 5 * 3 + (n_z - 1) * 5 * 4
         + 3 * (n_sp - 1) + n_sp + max(1, block // HEAD) * n_sp + 4
     )
     vmem = pltpu.VMEM
@@ -428,37 +457,47 @@
     new = new_query.shape[1]
     any_spec = pl.BlockSpec(memory_space=pl.ANY)
     vm_spec = pl.BlockSpec(memory_space=vmem)
-    cm, norm, top, read = pl.pallas_call(
+    cm, norm, top = pl.pallas_call(
         functools.partial(kernel, n_sp, n_tp, per_head, pad),
         out_shape=(
             jax.ShapeDtypeStruct((seqs, 2, per_head, HEAD, HEAD), BF),
             jax.ShapeDtypeStruct((seqs, 2, per_head, HEAD), F32),
             jax.ShapeDtypeStruct((seqs, 2, per_head, HEAD), F32),
-            jax.ShapeDtypeStruct((seqs, new, cols), BF),
         ),
-        in_specs=[any_spec] * 4 + [vm_spec] * 3,
-        out_specs=(any_spec, vm_spec, vm_spec, vm_spec),
+        in_specs=[any_spec] * 4 + [vm_spec] * 2,
+        out_specs=(any_spec, vm_spec, vm_spec),
         scratch_shapes=[
             vmem((n_tp, seg, width), BF),
-            vmem(slabs, BF), vmem(slabs, BF), vmem(slabs, BF), vmem(slabs, BF),
-            vmem((4, per_head, seg), F32), vmem((4, per_head, seg), F32), vmem((4, pad, seg), F32),
-            vmem((seg, cols), F32), vmem((seg, cols), F32), vmem((4 * pad, seg), F32),
+            vmem(slabs, BF), vmem(slabs, BF), vmem((2,) + slabs, BF),
+            vmem((4, per_head, seg), F32), vmem((4, per_head, seg), F32),
+            vmem((seg, cols), F32), vmem((seg, cols), F32), vmem((4 * heads_all, seg), F32),
+            vmem((4, pad, seg), F32),
             vmem((seg, cols), BF), vmem((seg, cols), BF),
             vmem((n_sp, 2, pad, HEAD), F32), vmem((2, pad, HEAD), F32),
             vmem((n_sp, 2 * pad, HEAD), F32), vmem((2 * pad, HEAD), F32),
             vmem((2, 2 * pad, HEAD), F32), vmem((2, 2 * pad, HEAD), F32),
             vmem((state_rows, HEAD), BF), vmem((n_sp, block, HEAD), BF), vmem((block, HEAD), BF),
             vmem((seqs, 2, per_head, HEAD, HEAD), BF),
-            dma((n_tp, 2)), dma((n_sp,)), dma((n_sp,)), dma((6,)), dma, dma((n_sp,)), dma((n_sp,)),
+            dma((n_tp, chunks)), dma((2, 2 * n_sp)), dma((6,)), dma, dma((n_sp,)), dma((n_sp,)),
             dma, dma((n_sp,)), dma((2,)), dma((n_send,)),
         ],
         compiler_params=pltpu.CompilerParams(
             collective_id=0, has_side_effects=True, vmem_limit_bytes=60 * 2**20
         ),
     )(
-        tokens, w_key.reshape(slabs), w_value.reshape(slabs), log_shift, gate_cols, bias, new_query
+        tokens, w_key.reshape(slabs), w_value.reshape(slabs), log_shift, gate_t, forget_bias
     )
-    return cm, norm, top[..., 0], read
+    return pl.pallas_call(
+        finish,
+        out_shape=(
+            jax.ShapeDtypeStruct(cm.shape, BF),
+            jax.ShapeDtypeStruct(norm.shape, F32),
+            jax.ShapeDtypeStruct(norm.shape[:3], F32),
+            jax.ShapeDtypeStruct((seqs, new, cols), BF),
+        ),
+        in_specs=[vm_spec] * 4,
+        out_specs=(vm_spec,) * 4,
+    )(cm, norm, top, new_query)
 
 
 def solution(mesh):

time: 141 us -> 132 us (0.936)
  local copies, waits for them, and re-layouts: 9.85 us -> 0 us
    unnamed x3 -> x0, local copies, waits for them, and re-layouts: 4.85 us -> none
    pallas_call x0 -> x1, Pallas kernels: none -> 2.39 us  [on_device(): pl.pallas_call(finish, out_shape=(jax.ShapeDtypeStruct(cm.shape, BF), jax...]
    dynamic_slice x2 -> x0, local copies, waits for them, and re-layouts: 2 us -> none  [pair(): lax.dynamic_slice_in_dim(array, k * per_head, per_head, axis)]
where the time goes in v2:
time: 132 us
  Pallas kernels  131 us (99%)
    pallas_call x1, Pallas kernels, on_device(): pl.pallas_call(functools.partial(kernel, n_sp, n_tp, per_head, pad), out_...  129 us

profile of v2, /device:TPU:0, one launch (start us, length us, event | category | flops | bytes accessed | tf_op | source)
XLA Modules:
  0.0 131.7 jit_solution(10780257126660821893)
XLA Ops:
  0.6 128.6 %shard_map.102 = (bf16[2,2,4,128,128]{4,3,2,1,0:T(8,128)(2,1)}, f32[2,2,4,128]{3,2,1,0:T(4,128)}, f32[2,2,4,128]{3,2,1,0:T(4,128)}) custom-call(bf16[2,768,1024]{2,1,0:T(8,128)(2,1)} %tok_in.1, bf16[16,256,512]{2,1,0:T(8,128)(2,1)} %bitcast.5, bf16[16,256,512]{2,1,0:T(8,128)(2,1)} %bitcast.6, f32[2,4,4,768]{3,2,1,0:T(4,128)} %shift_in.1, ...), custom_call_target="tpu_custom_call" | custom-call | tf_op jit(solution)/shard_map/pallas_call | solution.py:460
  129.3 2.4 %shard_map.103 = (bf16[2,2,4,128,128]{4,3,2,1,0:T(8,128)(2,1)}, f32[2,2,4,128]{3,2,1,0:T(4,128)}, f32[2,2,4]{2,1,0:T(2,128)}, bf16[2,128,512]{2,1,0:T(8,128)(2,1)}) custom-call(bf16[2,2,4,128,128]{4,3,2,1,0:T(8,128)(2,1)} %get-tuple-element.7.cm, f32[2,2,4,128]{3,2,1,0:T(4,128)} %get-tuple-element.8.norm, f32[2,2,4,128]{3,2,1,0:T(4,128)} %get-tuple-element.9.top, ...), custom_call_target="tpu_custom_call" | custom-call | tf_op jit(solution)/shard_map/pallas_call | solution.py:490

commit v3 on v2

--- a/solution.py
+++ b/solution.py
@@ -19,8 +19,8 @@
     tok_in, wk_in, wv_in, shift_in, wg, bias,
     cm_out, norm_out, max_out,
     tok, wk, wv, far_w, shift, shift_in2, acc_k, acc_v, gates, gate_rows, kp, vp,
-    stats, stat_own, norms, norm_own, pair_in, pair_own, st, rs, final, cm,
-    tok_sem, far_sem, local_sem, shift_sem, stat_sem, norm_sem, pair_sem, rs_sem, cm_sem,
+    stats, stat_own, norms, norm_own, pair_in, pair_own, st, chip, rs, final, cm,
+    tok_sem, far_sem, local_sem, shift_sem, stat_sem, norm_sem, pair_sem, chip_sem, rs_sem, cm_sem,
     send_sem,
 ):
     s = lax.axis_index("sp")
@@ -330,13 +330,25 @@
         mine = (row_of == index) | (row_of == index + pad)
         norm_own[...] = jnp.where(mine, n, norm_own[...])
 
+    def block_at(owner):
+        return pl.ds(pl.multiple_of(owner * block, block), block)
+
     def scatter(side):
-        for k in range(n_sp // 2):
-            owner = side * (n_sp // 2) + k
+        quarter = n_sp // 4
+        for m in range(quarter):
+            theirs = side * (n_sp // 2) + m * CORES + 1 - core
+            slot = side * quarter + m
+            send(st.at[block_at(theirs)], chip.at[slot], chip_sem.at[slot], sibling, t)
+        for m in range(quarter):
+            owner = side * (n_sp // 2) + m * CORES + core
+            slot = side * quarter + m
+            arrived(chip.at[slot], chip_sem.at[slot])
+            st[block_at(owner), :] = (
+                st[block_at(owner), :].astype(F32) + chip[slot].astype(F32)
+            ).astype(BF)
             send_if(
-                s != owner,
-                st.at[pl.ds(owner * block, block)],
-                rs.at[s], rs_sem.at[s], jnp.where(s == owner, sibling, owner), t,
+                s != owner, st.at[block_at(owner)], rs.at[z], rs_sem.at[z],
+                jnp.where(s == owner, sibling, owner), t,
             )
 
     for h in range(per_head):
@@ -356,8 +368,8 @@
     norms[s] = norm_own[...]
 
     summed = st[pl.ds(pl.multiple_of(s * block, block), block), :].astype(F32)
-    for d in range(1, n_sp):
-        frm = lax.rem(s + d, n_sp)
+    for d in range(1, n_z):
+        frm = lax.rem(z + d, n_z)
         arrived(rs.at[frm], rs_sem.at[frm])
         summed = summed + rs[frm].astype(F32)
     final[...] = summed.astype(BF)
@@ -476,10 +488,10 @@
             vmem((n_sp, 2, pad, HEAD), F32), vmem((2, pad, HEAD), F32),
             vmem((n_sp, 2 * pad, HEAD), F32), vmem((2 * pad, HEAD), F32),
             vmem((2, 2 * pad, HEAD), F32), vmem((2, 2 * pad, HEAD), F32),
-            vmem((state_rows, HEAD), BF), vmem((n_sp, block, HEAD), BF), vmem((block, HEAD), BF),
+            vmem((state_rows, HEAD), BF), vmem((n_sp // 2, block, HEAD), BF), vmem((n_z, block, HEAD), BF), vmem((block, HEAD), BF),
             vmem((seqs, 2, per_head, HEAD, HEAD), BF),
             dma((n_tp, chunks)), dma((2, 2 * n_sp)), dma((6,)), dma, dma((n_sp,)), dma((n_sp,)),
-            dma, dma((n_sp,)), dma((2,)), dma((n_send,)),
+            dma, dma((n_sp // 2,)), dma((n_z,)), dma((2,)), dma((n_send,)),
         ],
         compiler_params=pltpu.CompilerParams(
             collective_id=0, has_side_effects=True, vmem_limit_bytes=60 * 2**20

time: 132 us -> 124 us (0.939)
  Pallas kernels: 131 us -> 123 us
    pallas_call x1, Pallas kernels: 129 us -> 121 us  [on_device(): pl.pallas_call(functools.partial(kernel, n_sp, n_tp, per_head, pad), out_...]
where the time goes in v3:
time: 124 us
  Pallas kernels  123 us (99%)
    pallas_call x1, Pallas kernels, on_device(): pl.pallas_call(functools.partial(kernel, n_sp, n_tp, per_head, pad), out_...  121 us

profile of v3, /device:TPU:0, one launch (start us, length us, event | category | flops | bytes accessed | tf_op | source)
XLA Modules:
  0.0 124.1 jit_solution(11731227351708219506)
XLA Ops:
  0.6 121.1 %shard_map.102 = (bf16[2,2,4,128,128]{4,3,2,1,0:T(8,128)(2,1)}, f32[2,2,4,128]{3,2,1,0:T(4,128)}, f32[2,2,4,128]{3,2,1,0:T(4,128)}) custom-call(bf16[2,768,1024]{2,1,0:T(8,128)(2,1)} %tok_in.1, bf16[16,256,512]{2,1,0:T(8,128)(2,1)} %bitcast.5, bf16[16,256,512]{2,1,0:T(8,128)(2,1)} %bitcast.6, f32[2,4,4,768]{3,2,1,0:T(4,128)} %shift_in.1, ...), custom_call_target="tpu_custom_call" | custom-call | tf_op jit(solution)/shard_map/pallas_call | solution.py:472
  121.7 2.4 %shard_map.103 = (bf16[2,2,4,128,128]{4,3,2,1,0:T(8,128)(2,1)}, f32[2,2,4,128]{3,2,1,0:T(4,128)}, f32[2,2,4]{2,1,0:T(2,128)}, bf16[2,128,512]{2,1,0:T(8,128)(2,1)}) custom-call(bf16[2,2,4,128,128]{4,3,2,1,0:T(8,128)(2,1)} %get-tuple-element.7.cm, f32[2,2,4,128]{3,2,1,0:T(4,128)} %get-tuple-element.8.norm, f32[2,2,4,128]{3,2,1,0:T(4,128)} %get-tuple-element.9.top, ...), custom_call_target="tpu_custom_call" | custom-call | tf_op jit(solution)/shard_map/pallas_call | solution.py:502
